TPU v7x, 32 devices: a whole 2x2x4 slice. The times are simulated.
32 devices in a mesh: sp: 16 (over z, y, core), tp: 2 (over x).
Axes of the slice: x: 2, y: 2, z: 4, core: 2. Of those that a mesh axis runs over, the one named last changes fastest.
Arguments:
- tokens: bfloat16 [6144, 2048], P('sp', 'tp'), may hold values from -60 to 60
- pre_gain: bfloat16 [2048], P('tp'), may hold values from 0.099609375 to 1.8984375
- w_query: bfloat16 [2048, 1024], P('sp', 'tp'), may hold values from -1 to 1
- w_key: bfloat16 [2048, 1024], P('sp', 'tp'), may hold values from -1 to 1
- w_value: bfloat16 [2048, 1024], P('sp', 'tp'), may hold values from -0.125 to 0.125
- w_pool: bfloat16 [2048, 1024], P('sp', 'tp'), may hold values from -0.125 to 0.125
- lambdas: float32 [8], P('tp'), may hold values from 0.3 to 0.8
- sub_gain: float32 [128], replicated, may hold values from 0.1 to 1.9
- group_weight: bfloat16 [8, 128, 128], P('tp'), may hold values from -0.5 to 0.5
- pool_scale: float32 [1024], P('tp'), may hold values from 0.1 to 1.9
- w_out: bfloat16 [2048, 2048], P('tp', 'sp'), may hold values from -0.125 to 0.125
Outputs:
- mixed_out: bfloat16 [6144, 2048], P(('sp', 'tp'))
All inputs are finite; a program needn't handle non-finite values.
Results may differ from a plain program's by a relative error of at most 0.015.
Values may be sent and summed in bfloat16 or wider, within the bound.
No kernel may reach another device: no remote copies, remote signals or barrier semaphores. Data moves between devices by JAX's collectives and lax.ppermute only.
A program may use at most 128 MiB of HBM per device.

v0:
```python
import math

import jax
import jax.numpy as jnp
from jax import lax
from jax.sharding import PartitionSpec as P

EPSILON = 1e-06
NEG_LARGE = -1e30
WINDOWS = (2, 4, 8, 16)
RIM_ROWS = 15


def passed_along(block, axis, distance):
    devices = range(lax.axis_size(axis))
    route = [(i - distance, i) for i in devices if i - distance in devices]
    return lax.ppermute(block, axis, route)


def unchanged(carried):
    return carried


def local(
    tokens,
    pre_gain,
    w_query,
    w_key,
    w_value,
    w_pool,
    lambdas,
    sub_gain,
    group_weight,
    pool_scale,
    w_out,
):
    tok_rows = tokens.shape[0]
    model_width = tokens.shape[1] * lax.axis_size("tp")
    local_heads = lambdas.shape[0]
    head_dim = w_query.shape[1] // (2 * local_heads)
    value_dim = w_value.shape[1] // local_heads
    local_groups = group_weight.shape[0]
    group_dim = group_weight.shape[1]
    q_cols = w_query.shape[1]
    v_cols = w_value.shape[1]
    w_cat = jnp.concatenate([w_query, w_key, w_value, w_pool], axis=1)
    w_in_full, w_out_rows = (
        lax.all_gather(w_cat, "sp", axis=0, tiled=True),
        lax.all_gather(w_out, "sp", axis=1, tiled=True),
    )
    gain_row = pre_gain.reshape(1, -1)
    pieces = (
        lax.all_gather(tokens, "tp", axis=1, tiled=True),
        lax.all_gather(gain_row, "tp", axis=1, tiled=True),
    )
    feature_part = pieces[0].astype(jnp.float32)
    scaled = (feature_part * pieces[1].astype(jnp.float32)).astype(jnp.bfloat16)
    projection = jnp.dot(scaled, w_in_full, preferred_element_type=jnp.float32)
    projection, squares = (projection, jnp.sum(feature_part * feature_part, axis=1))
    inverse = lax.rsqrt(squares / model_width + EPSILON)
    projected = (projection * inverse[:, None]).astype(jnp.bfloat16)
    queries = projected[:, :q_cols].reshape(tok_rows, local_heads, 2, head_dim)
    key_rows = projected[:, q_cols : 2 * q_cols]
    values = projected[:, 2 * q_cols : 2 * q_cols + v_cols]
    pool_in = projected[:, 2 * q_cols + v_cols :]
    first_row = lax.axis_index("sp") * tok_rows
    positions = first_row + jnp.arange(tok_rows, dtype=jnp.int32)
    shard_group = tok_rows * max(1, 1024 // tok_rows)
    score_scale = 1.0 / math.sqrt(head_dim)
    last_query = first_row + tok_rows - 1
    initial_max = jnp.full((local_heads, 2, tok_rows), NEG_LARGE, jnp.float32)
    initial_sum = jnp.zeros((local_heads, 2, tok_rows), jnp.float32)
    initial_weighted = jnp.zeros((local_heads, 2, tok_rows, value_dim), jnp.float32)
    pieces = (
        lax.all_gather(key_rows, "sp", axis=0, tiled=True),
        lax.all_gather(values, "sp", axis=0, tiled=True),
    )
    key_piece = pieces[0].reshape(-1, local_heads, 2, head_dim)
    value_piece = pieces[1].reshape(-1, local_heads, value_dim)
    length = key_piece.shape[0]
    block_len = math.gcd(length, shard_group)

    def one_block(block_index, state):
        block_start = block_index * block_len

        def compute(inner):
            running_max, running_sum, weighted = inner
            key_block = lax.dynamic_slice_in_dim(key_piece, block_start, block_len, 0)
            value_block = lax.dynamic_slice_in_dim(value_piece, block_start, block_len, 0)
            scores = (
                jnp.einsum(
                    "qhmd,khmd->hmqk", queries, key_block, preferred_element_type=jnp.float32
                )
                * score_scale
            )
            key_pos = block_start + jnp.arange(block_len, dtype=jnp.int32)
            allowed = key_pos[None, :] <= positions[:, None]
            scores = jnp.where(allowed, scores, NEG_LARGE)
            new_max = jnp.maximum(running_max, jnp.max(scores, axis=-1))
            factor = jnp.exp(running_max - new_max)
            expo = jnp.where(allowed, jnp.exp(scores - new_max[..., None]), 0.0)
            running_sum = running_sum * factor + jnp.sum(expo, axis=-1)
            weighted = weighted * factor[..., None] + jnp.einsum(
                "hmqk,khd->hmqd",
                expo.astype(jnp.bfloat16),
                value_block,
                preferred_element_type=jnp.float32,
            )
            return (new_max, running_sum, weighted)

        return lax.cond(block_start <= last_query, compute, unchanged, state)

    running_max, running_sum, weighted = lax.fori_loop(
        0, length // block_len, one_block, (initial_max, initial_sum, initial_weighted)
    )
    head_mix = (
        weighted[:, 0] / running_sum[:, 0, :, None]
        - lambdas[:, None, None] * weighted[:, 1] / running_sum[:, 1, :, None]
    )
    mean_sq = jnp.mean(head_mix * head_mix, axis=-1, keepdims=True)
    normed = head_mix * lax.rsqrt(mean_sq + EPSILON) * sub_gain
    attention = jnp.transpose(normed, (1, 0, 2)).astype(jnp.bfloat16)
    halo_rows = passed_along(pool_in[tok_rows - RIM_ROWS :], "sp", 1)
    extended = jnp.concatenate([halo_rows, pool_in], axis=0).astype(jnp.float32)
    running = jnp.concatenate(
        [jnp.zeros((1, extended.shape[1]), jnp.float32), jnp.cumsum(extended, axis=0)], axis=0
    )
    running_top = running[RIM_ROWS + 1 :]
    window_ids = (
        lax.axis_index("tp") * local_groups + jnp.arange(local_groups, dtype=jnp.int32)
    ) % len(WINDOWS)
    column_window = jnp.repeat(window_ids, group_dim)
    average = jnp.zeros_like(running_top)
    for window_slot, window_span in enumerate(WINDOWS):
        running_low = running[RIM_ROWS + 1 - window_span : RIM_ROWS + 1 - window_span + tok_rows]
        window_count = jnp.minimum(positions + 1, window_span).astype(jnp.float32)
        average = average + jnp.where(
            column_window[None, :] == window_slot,
            (running_top - running_low) / window_count[:, None],
            0.0,
        )
    differ = (
        (average - pool_in.astype(jnp.float32))
        .astype(jnp.bfloat16)
        .reshape(tok_rows, local_groups, group_dim)
    )
    pooled = jnp.einsum("tgc,gcd->tgd", differ, group_weight, preferred_element_type=jnp.float32)
    pooled = (pooled * pool_scale.reshape(local_groups, group_dim)).astype(jnp.bfloat16)
    branch = jnp.concatenate([attention, pooled], axis=2).reshape(tok_rows, -1)
    return lax.psum_scatter(
        jnp.dot(branch, w_out_rows, preferred_element_type=jnp.float32).astype(jnp.bfloat16),
        "tp",
        scatter_dimension=0,
        tiled=True,
    )


def solution(mesh):
    placed = (
        P("sp", "tp"),
        P("tp"),
        P("sp", "tp"),
        P("sp", "tp"),
        P("sp", "tp"),
        P("sp", "tp"),
        P("tp"),
        P(),
        P("tp", None, None),
        P("tp"),
        P("tp", "sp"),
    )
    return jax.shard_map(
        local, mesh=mesh, in_specs=placed, out_specs=P(("sp", "tp"), None), check_vma=False
    )
```

profile of v0, /device:TPU:0, one launch (start us, length us, event | category | flops | bytes accessed | tf_op | source)
XLA Modules:
  0.0 377.3 jit_solution(12847883650176811688)
XLA Ops:
  6.5 0.7 all-gather.7.cloned.1.call-update
  7.3 1.9 pad_maximum_fusion.1
  9.3 5.5 %all-gather = bf16[2048]{0:T(1024)(128)(2,1)S(1)} all-gather(bf16[1024]{0:T(1024)(128)(2,1)} %param.16), channel_id=2, replica_groups=mesh['sp'=16,'tp'=2] {'tp'}, dimensions={0}, use_global_device_ids=true | all-gather | bytes 6144 | tf_op jit(solution)/shard_map/all_gather | solution.py:54
  14.8 24.0 %all-gather.7.cloned.1.call-done = bf16[384,2048]{1,0:T(8,128)(2,1)} async-done(((bf16[384,1024]{1,0:T(8,128)(2,1)}), bf16[384,2048]{1,0:T(8,128)(2,1)}) %all-gather.7.cloned.1.call-update) | async-done | bytes 1572880 | tf_op jit(solution)/shard_map/all_gather | solution.py:53
  38.8 1.8 fusion.20
  40.6 74.7 %all-gather.9.cloned.1.call-done = bf16[2048,2048]{1,0:T(8,128)(2,1)} async-done(((bf16[128,2048]{1,0:T(8,128)(2,1)}), bf16[2048,2048]{1,0:T(8,128)(2,1)}) %all-gather.9.cloned.1.call-update) | async-done | bytes 8388624 | tf_op jit(solution)/shard_map/all_gather | solution.py:48
  115.3 7.3 %multiply_convert_fusion = bf16[384,2048]{1,0:T(8,128)(2,1)S(1)} fusion(bf16[2048,2048]{1,0:T(8,128)(2,1)} %all-gather.9.cloned.1.call-done, bf16[384,2048]{1,0:T(8,128)(2,1)} %all-gather.7.cloned.1.call-done, f32[2048]{0:T(1024)S(1)} %mul.112, f32[384]{0:T(512)S(1)} %add_rsqrt_fusion.1), kind=kOutput, calls=%fused_computation.28 | convolution fusion | flops 3225157632 | bytes 11544064 | tf_op jit(solution)/shard_map/dot_general | solution.py:58
  122.6 1.0 fusion.51
  123.7 0.5 all-gather.13.cloned.1.call-update
  124.3 0.5 all-gather.15.cloned.1.call-update
  125.2 2.1 collective-permute-start
  127.4 0.2 copy.34
  127.6 0.6 collective-permute-done
  128.5 0.7 fusion.25
  129.3 0.3 copy.39
  129.7 1.7 fusion.24
  131.5 52.3 %all-gather.11.cloned.1.call-done = bf16[6144,512]{1,0:T(8,128)(2,1)} async-done(((bf16[384,512]{1,0:T(8,128)(2,1)}), bf16[6144,512]{1,0:T(8,128)(2,1)}) %all-gather.11.cloned.1.call-update) | async-done | bytes 6291472 | tf_op jit(solution)/shard_map/all_gather | solution.py:75
  183.8 8.7 %copy.33 = bf16[6144,512]{0,1:T(8,128)(2,1)} copy(bf16[6144,512]{1,0:T(8,128)(2,1)} %all-gather.11.cloned.1.call-done) | data formatting | bytes 12582912 | tf_op jit(solution)/shard_map/all_gather | solution.py:75
  192.5 53.6 %all-gather.13.cloned.1.call-done = bf16[6144,512]{1,0:T(8,128)(2,1)} async-done(((bf16[384,512]{1,0:T(8,128)(2,1)}), bf16[6144,512]{1,0:T(8,128)(2,1)}) %all-gather.13.cloned.1.call-update) | async-done | bytes 6291472 | tf_op jit(solution)/shard_map/all_gather | solution.py:76
  246.0 6.5 %copy_bitcast_fusion = bf16[6144,4,128]{2,0,1:T(8,128)(2,1)} fusion(bf16[6144,512]{1,0:T(8,128)(2,1)} %all-gather.13.cloned.1.call-done), kind=kLoop, calls=%fused_computation.23 | loop fusion | bytes 12582912
  252.7 11.3 %while.18 = (s32[]{:T(128)}, f32[4,2,384]{2,1,0:T(2,128)S(1)}, f32[4,2,384]{2,1,0:T(2,128)S(1)}, f32[4,2,384,128]{3,2,1,0:T(8,128)S(1)}, s32[]{:T(128)}, /*index...) while((s32[]{:T(128)}, f32[4,2,384]{2,1,0:T(2,128)S(1)}, ...), condition=%wide.region_6.7_spmd.clone, body=%wide.region_1.6_spmd.clone.sunk | while | flops 937729152 | bytes 34812224 | solution.py:113
  252.7 10.6 %conditional.3 = ((f32[4,2,384]{2,1,0:T(2,128)S(1)}, f32[4,2,384]{2,1,0:T(2,128)S(1)}, f32[4,2,384,128]{3,2,1,0:T(8,128)S(1)})) conditional(s32[]{:T(128)} %convert_element_type.123, (f32[4,2,384]{2,1,0:T(2,128)S(1)}, f32[4,2,384]{2,1,0:T(2,128)S(1)}, f32[4,2,384,128]{3,2,1,0:T(8,128)S(1)}) %tuple.58, (s32[]{:T(128)}, s32[]{:T(128)}, ...), branch_computations={%region_2.0_spmd, %region_3.5_spmd} | conditional | flops 937729152 | bytes 34810448 | solution.py:111
  252.7 0.2 broadcast_compare_fusion
  253.0 2.8 fusion.2
  255.8 2.3 fusion.4
  258.1 5.2 %multiply_add_fusion = f32[4,2,384,128]{3,2,1,0:T(8,128)S(1)} fusion(f32[4,2,384,128]{3,2,1,0:T(8,128)S(1)} %get-tuple-element.182, f32[4,2,768,384]{3,2,1,0:T(8,128)S(1)} %get-tuple-element.278, f32[4,2,384]{2,1,0:T(2,128)S(1)} %max.2, pred[384,768]{0,1:T(8,128)(4,1)S(1)} %broadcast_compare_fusion, bf16[6144,4,128]{2,0,1:T(8,128)(2,1)} %get-tuple-element.183, ...), kind=kOutput, calls=%fused_computation.8 | convolution fusion | flops 616562688 | bytes 13688836 | tf_op jit(solution)/shard_map/while/body/eval_jaxpr/cond/branch_1_fun/hmqk,khd->hmqd/dot_general | solution.py:103
  264.0 0.5 copy.36
  264.5 0.2 multiply_reduce_fusion
  264.9 1.1 pad_maximum_fusion
  266.0 33.3 %all-gather.15.cloned.1.call-done = bf16[1024,2048]{1,0:T(8,128)(2,1)} async-done(((bf16[1024,128]{1,0:T(8,128)(2,1)}), bf16[1024,2048]{1,0:T(8,128)(2,1)}) %all-gather.15.cloned.1.call-update) | async-done | bytes 4194320 | tf_op jit(solution)/shard_map/all_gather | solution.py:49
  299.3 5.2 %convolution_convert_fusion = bf16[384,2048]{1,0:T(8,128)(2,1)} fusion(bf16[384,1024]{0,1:T(8,128)(2,1)S(1)} %bitcast.99, bf16[1024,2048]{1,0:T(8,128)(2,1)} %all-gather.15.cloned.1.call-done), kind=kOutput, calls=%fused_computation.29 | convolution fusion | flops 1611399168 | bytes 6553600 | tf_op jit(solution)/shard_map/dot_general | solution.py:151
  304.5 66.0 %reduce-scatter.2.cloned.1.call-done = bf16[192,2048]{1,0:T(8,128)(2,1)} async-done(((bf16[384,2048]{1,0:T(8,128)(2,1)}), bf16[192,2048]{1,0:T(8,128)(2,1)}) %reduce-scatter.2.cloned.1.call-update) | async-done | bytes 786448 | tf_op jit(solution)/shard_map/reduce_scatter | solution.py:150
  (66 shorter events, 1.5 us)
Async XLA Ops:
  6.5 123.2 %copy-start = (bf16[4,128,128]{2,1,0:T(8,128)(2,1)S(1)}, bf16[4,128,128]{2,1,0:T(8,128)(2,1)}, u32[]{:S(2)}) copy-start(bf16[4,128,128]{2,1,0:T(8,128)(2,1)} %param.23) | copy-start | bytes 393220
  6.5 32.3 %all-gather.7.cloned.1.call-start = ((), (), s32[]{:S(2)}) async-start(), calls=%async_computation.1 | async-start | bytes 2359296 | tf_op jit(solution)/shard_map/all_gather | solution.py:53
  7.3 108.0 %all-gather.9.cloned.1.call-start = ((), (), s32[]{:S(2)}) async-start(), calls=%async_computation.2 | async-start | bytes 8912896 | tf_op jit(solution)/shard_map/all_gather | solution.py:48
  9.3 174.5 %all-gather.11.cloned.1.call-start = ((), (), s32[]{:S(2)}) async-start(), calls=%async_computation.3 | async-start | bytes 6684672 | tf_op jit(solution)/shard_map/all_gather | solution.py:75
  123.6 122.4 %all-gather.13.cloned.1.call-start = ((), (), s32[]{:S(2)}) async-start(), calls=%async_computation.4 | async-start | bytes 6684672 | tf_op jit(solution)/shard_map/all_gather | solution.py:76
  124.2 175.0 %all-gather.15.cloned.1.call-start = ((), (), s32[]{:S(2)}) async-start(), calls=%async_computation.5 | async-start | bytes 4456448 | tf_op jit(solution)/shard_map/all_gather | solution.py:49
  124.8 245.7 %reduce-scatter.2.cloned.1.call-start = ((), (), s32[]{:S(2)}) async-start(), calls=%async_computation.6 | async-start | bytes 2359296 | tf_op jit(solution)/shard_map/reduce_scatter | solution.py:150
  125.2 3.0 collective-permute-start
  128.5 1.3 copy-start.4
  252.7 11.9 %copy-start.2 = (f32[4]{0:T(128)S(1)}, f32[4]{0:T(128)}, u32[]{:S(2)}) copy-start(f32[4]{0:T(128)} %param.21) | copy-start | bytes 52
  264.0 0.8 copy-start.3
  299.3 71.2 %copy-start.1 = (bf16[4,128,128]{2,1,0:T(8,128)(2,1)S(1)}, bf16[4,128,128]{2,1,0:T(8,128)(2,1)}, u32[]{:S(2)}) copy-start(bf16[4,128,128]{2,1,0:T(8,128)(2,1)} %param.23) | copy-start | bytes 393220
Sparse Core Ops, SparseCore 0:
  8.9 29.8 all-gather.6
  41.0 74.2 all-gather.8
  123.8 59.9 all-gather.10
  185.9 60.0 all-gather.12
  248.0 51.1 all-gather.14
  304.6 65.8 reduce-scatter.1
where the time goes:
time: 378 us; the launch traced here: 377 us
  waiting for transfers between devices  306 us (81%)
  matrix products  22.3 us (6%)
  local copies, waits for them, and re-layouts  17.8 us (5%)
  between operations  13.7 us (4%)
  other arithmetic  8.77 us (2%)
  blocking collectives  5.5 us (1%)
    all_gather x1, waiting for transfers between devices, local(): lax.all_gather(w_cat, 'sp', axis=0, tiled=True)  74.7 us
    reduce_scatter x1, waiting for transfers between devices, local(): lax.psum_scatter(jnp.dot(branch, w_out_rows, preferred_element_type=jnp.f...  66 us
    all_gather x1, waiting for transfers between devices, local(): lax.all_gather(values, 'sp', axis=0, tiled=True)  53.6 us
    all_gather x1, waiting for transfers between devices, local(): lax.all_gather(key_rows, 'sp', axis=0, tiled=True)  52.3 us
    all_gather x1, waiting for transfers between devices, local(): lax.all_gather(w_out, 'sp', axis=1, tiled=True)  33.3 us
    all_gather x1, waiting for transfers between devices, local(): lax.all_gather(tokens, 'tp', axis=1, tiled=True)  24 us
    all_gather x1, local copies, waits for them, and re-layouts, local(): lax.all_gather(key_rows, 'sp', axis=0, tiled=True)  8.7 us
  transfers between devices with their start and end apart: 7, of which 7 were waited for; matrix products, arithmetic and copies ran while one was open for 9% of the time, Pallas kernels for 0%

commit v1 on v0

v1 whole, which is shorter than its diff:
```python
import functools
import math

import jax
import jax.numpy as jnp
from jax import lax
from jax.experimental import pallas as pl
from jax.experimental.pallas import tpu as pltpu
from jax.sharding import PartitionSpec as P

EPSILON = 1e-06
NEG_LARGE = -1e30
WINDOWS = (2, 4, 8, 16)
RIM_ROWS = 15


def passed_along(block, axis, distance):
    devices = range(lax.axis_size(axis))
    route = [(i - distance, i) for i in devices if i - distance in devices]
    return lax.ppermute(block, axis, route)


def swapped(block, axis):
    return lax.ppermute(block, axis, [(0, 1), (1, 0)])


def attention_kernel(
    place_ref, lam_ref, gain_ref, q_ref, kv_ref, out_ref, max_ref, acc_ref, *, inner, head_dim
):
    rows = q_ref.shape[2]
    value_dim = out_ref.shape[3]
    pair = 2 * head_dim
    scale = math.log2(math.e) / math.sqrt(head_dim)
    query_block = pl.program_id(1) * inner + place_ref[0]
    query = q_ref[0, 0]
    lane = lax.broadcasted_iota(jnp.int32, (rows, pair), 1)
    blank = jnp.zeros_like(query)
    both = jnp.concatenate(
        [jnp.where(lane < head_dim, query, blank), jnp.where(lane < head_dim, blank, query)], axis=0
    )
    ones = jnp.ones((rows, value_dim), jnp.bfloat16)

    def scores_of(block):
        keys = kv_ref[block % inner, block // inner, 0, :, :pair]
        return scale * lax.dot_general(
            both, keys, (((1,), (1,)), ((), ())), preferred_element_type=jnp.float32
        )

    def weighted_of(block, expo):
        values = kv_ref[block % inner, block // inner, 0, :, pair:]
        return jnp.dot(
            expo.astype(jnp.bfloat16),
            jnp.concatenate([values, ones], axis=1),
            preferred_element_type=jnp.float32,
        )

    scores = scores_of(query_block)
    row = lax.broadcasted_iota(jnp.int32, scores.shape, 0)
    column = lax.broadcasted_iota(jnp.int32, scores.shape, 1)
    row = jnp.where(row >= rows, row - rows, row)
    scores = jnp.where(column <= row, scores, NEG_LARGE)
    first_max = jnp.max(scores, axis=1, keepdims=True)
    max_ref[...] = jnp.broadcast_to(first_max, max_ref.shape)
    acc_ref[...] = weighted_of(query_block, jnp.exp2(scores - first_max))

    def step(block, carry):
        scores = scores_of(block)
        old_max = max_ref[:, :1]
        new_max = jnp.maximum(old_max, jnp.max(scores, axis=1, keepdims=True))
        expo = jnp.exp2(scores - new_max)
        max_ref[...] = jnp.broadcast_to(new_max, max_ref.shape)
        acc_ref[...] = acc_ref[...] * jnp.exp2(old_max - new_max) + weighted_of(block, expo)
        return carry

    lax.fori_loop(0, query_block, step, 0)
    head_mix = (
        acc_ref[:rows, :value_dim] / acc_ref[:rows, value_dim:]
        - lam_ref[pl.program_id(0)]
        * acc_ref[rows:, :value_dim]
        / acc_ref[rows:, value_dim:]
    )
    mean_sq = jnp.mean(head_mix * head_mix, axis=1, keepdims=True)
    normed = head_mix * lax.rsqrt(mean_sq + EPSILON) * gain_ref[...]
    out_ref[0, 0] = normed.astype(jnp.bfloat16)


def attend(place, lam, gain, queries, kv, head_dim):
    spread, heads, rows, _ = queries.shape
    inner = kv.shape[0]
    value_dim = kv.shape[4] - 2 * head_dim
    smem = pl.BlockSpec(memory_space=pltpu.SMEM)
    return pl.pallas_call(
        functools.partial(attention_kernel, inner=inner, head_dim=head_dim),
        grid=(heads, spread),
        in_specs=[
            smem,
            smem,
            pl.BlockSpec((1, value_dim), lambda h, j: (0, 0)),
            pl.BlockSpec((1, 1, rows, 2 * head_dim), lambda h, j: (j, h, 0, 0)),
            pl.BlockSpec((inner, spread, 1, rows, kv.shape[4]), lambda h, j: (0, 0, h, 0, 0)),
        ],
        out_specs=pl.BlockSpec((1, 1, rows, value_dim), lambda h, j: (j, h, 0, 0)),
        out_shape=jax.ShapeDtypeStruct((spread, heads, rows, value_dim), jnp.bfloat16),
        scratch_shapes=[
            pltpu.VMEM((2 * rows, 128), jnp.float32),
            pltpu.VMEM((2 * rows, 2 * value_dim), jnp.float32),
        ],
        compiler_params=pltpu.CompilerParams(
            dimension_semantics=("arbitrary", "arbitrary"), vmem_limit_bytes=56 << 20
        ),
        cost_estimate=pl.CostEstimate(
            flops=spread * heads * rows * rows * inner * spread * 1024,
            transcendentals=spread * heads * rows * rows * inner * spread,
            bytes_accessed=kv.size * 2,
        ),
        name="diff_attention",
    )(place, lam, gain, queries, kv)


def exchanged(blocks, groups):
    return lax.all_to_all(
        blocks, "sp", split_axis=0, concat_axis=0, tiled=True, axis_index_groups=groups
    )


def local(
    tokens,
    pre_gain,
    w_query,
    w_key,
    w_value,
    w_pool,
    lambdas,
    sub_gain,
    group_weight,
    pool_scale,
    w_out,
):
    tok_rows = tokens.shape[0]
    model_width = tokens.shape[1] * lax.axis_size("tp")
    local_heads = lambdas.shape[0]
    head_dim = w_query.shape[1] // (2 * local_heads)
    value_dim = w_value.shape[1] // local_heads
    local_groups = group_weight.shape[0]
    group_dim = group_weight.shape[1]
    q_cols = w_query.shape[1]
    v_cols = w_value.shape[1]
    sp_size = lax.axis_size("sp")
    tp_size = lax.axis_size("tp")
    spread = math.gcd(local_heads, sp_size)
    inner = sp_size // spread
    heads_here = local_heads // spread
    apart = [[r + inner * j for j in range(spread)] for r in range(inner)]
    beside = [[r + inner * j for r in range(inner)] for j in range(spread)]
    my_sp = lax.axis_index("sp")
    my_tp = lax.axis_index("tp")
    w_cat = jnp.concatenate([w_query, w_key, w_value, w_pool], axis=1)
    w_in_full = lax.all_gather(w_cat, "sp", axis=0, tiled=True)
    gain_row = pre_gain.reshape(1, -1)
    if tp_size == 2:
        other = swapped(tokens, "tp")
        pieces = jnp.where(
            my_tp == 0,
            jnp.concatenate([tokens, other], axis=1),
            jnp.concatenate([other, tokens], axis=1),
        )
    else:
        pieces = lax.all_gather(tokens, "tp", axis=1, tiled=True)
    gains = lax.all_gather(gain_row, "tp", axis=1, tiled=True)
    feature_part = pieces.astype(jnp.float32)
    scaled = (feature_part * gains.astype(jnp.float32)).astype(jnp.bfloat16)
    squares = jnp.sum(feature_part * feature_part, axis=1)
    inverse = lax.rsqrt(squares / model_width + EPSILON)
    projection = jnp.dot(scaled, w_in_full, preferred_element_type=jnp.float32)
    projected = (projection * inverse[:, None]).astype(jnp.bfloat16)
    pair = 2 * head_dim
    queries = jnp.stack([projected[:, h * pair : (h + 1) * pair] for h in range(local_heads)])
    kv = jnp.stack(
        [
            jnp.concatenate(
                [
                    projected[:, q_cols + h * pair : q_cols + (h + 1) * pair],
                    projected[:, 2 * q_cols + h * value_dim : 2 * q_cols + (h + 1) * value_dim],
                ],
                axis=1,
            )
            for h in range(local_heads)
        ]
    )
    pool_in = projected[:, 2 * q_cols + v_cols :]
    positions = my_sp * tok_rows + jnp.arange(tok_rows, dtype=jnp.int32)
    if spread > 1:
        kv = exchanged(kv, apart)
        queries = exchanged(queries, apart)
    kv = kv.reshape(-1, kv.shape[2])
    kv = lax.all_gather(kv, "sp", axis=0, tiled=True, axis_index_groups=beside)
    kv = kv.reshape(inner, spread, heads_here, tok_rows, pair + value_dim)
    queries = queries.reshape(spread, heads_here, tok_rows, pair)
    lam = lax.dynamic_slice_in_dim(lambdas, (my_sp // inner) * heads_here, heads_here)
    place = (my_sp % inner).astype(jnp.int32).reshape(1)
    attention = attend(place, lam, sub_gain.reshape(1, -1), queries, kv, head_dim)
    attention = attention.reshape(local_heads, tok_rows, value_dim)
    if spread > 1:
        attention = exchanged(attention, apart)
    attention = jnp.transpose(attention, (1, 0, 2))
    halo_rows = passed_along(pool_in[tok_rows - RIM_ROWS :], "sp", 1)
    extended = jnp.concatenate([halo_rows, pool_in], axis=0).astype(jnp.float32)
    running = jnp.concatenate(
        [jnp.zeros((1, extended.shape[1]), jnp.float32), jnp.cumsum(extended, axis=0)], axis=0
    )
    running_top = running[RIM_ROWS + 1 :]
    window_ids = (
        lax.axis_index("tp") * local_groups + jnp.arange(local_groups, dtype=jnp.int32)
    ) % len(WINDOWS)
    column_window = jnp.repeat(window_ids, group_dim)
    average = jnp.zeros_like(running_top)
    for window_slot, window_span in enumerate(WINDOWS):
        running_low = running[RIM_ROWS + 1 - window_span : RIM_ROWS + 1 - window_span + tok_rows]
        window_count = jnp.minimum(positions + 1, window_span).astype(jnp.float32)
        average = average + jnp.where(
            column_window[None, :] == window_slot,
            (running_top - running_low) / window_count[:, None],
            0.0,
        )
    differ = (
        (average - pool_in.astype(jnp.float32))
        .astype(jnp.bfloat16)
        .reshape(tok_rows, local_groups, group_dim)
    )
    pooled = jnp.einsum("tgc,gcd->tgd", differ, group_weight, preferred_element_type=jnp.float32)
    pooled = (pooled * pool_scale.reshape(local_groups, group_dim)).astype(jnp.bfloat16)
    branch = jnp.concatenate([attention, pooled], axis=2).reshape(tok_rows, -1)
    w_out_t = lax.all_gather(w_out.T, "sp", axis=0, tiled=True)

    def out_of(rows):
        return lax.dot_general(
            rows, w_out_t, (((1,), (1,)), ((), ())), preferred_element_type=jnp.float32
        )

    if tp_size == 2:
        half = tok_rows // 2
        sent = out_of(lax.dynamic_slice_in_dim(branch, (1 - my_tp) * half, half))
        arrived = swapped(sent.astype(jnp.bfloat16), "tp")
        kept = out_of(lax.dynamic_slice_in_dim(branch, my_tp * half, half))
        return (kept + arrived.astype(jnp.float32)).astype(jnp.bfloat16)
    return lax.psum_scatter(
        out_of(branch).astype(jnp.bfloat16), "tp", scatter_dimension=0, tiled=True
    )


def solution(mesh):
    placed = (
        P("sp", "tp"),
        P("tp"),
        P("sp", "tp"),
        P("sp", "tp"),
        P("sp", "tp"),
        P("sp", "tp"),
        P("tp"),
        P(),
        P("tp", None, None),
        P("tp"),
        P("tp", "sp"),
    )
    return jax.shard_map(
        local, mesh=mesh, in_specs=placed, out_specs=P(("sp", "tp"), None), check_vma=False
    )
```

time: 378 us -> 240 us (0.63)
  waiting for transfers between devices: 306 us -> 113 us
  blocking collectives: 5.5 us -> 41.9 us
  Pallas kernels: 0 us -> 29.2 us
  local copies, waits for them, and re-layouts: 17.8 us -> 5.14 us
  starting transfers between devices: 2.35 us -> 14 us
  matrix products: 22.3 us -> 16.2 us
    all_gather x5 -> x3, waiting for transfers between devices: 238 us -> 68.4 us  [the longest x1 55 us: local(): w_in_full = lax.all_gather(w_cat, 'sp', axis=0, tiled=True)]
    reduce_scatter x1 -> x0, waiting for transfers between devices: 66 us -> none  [local(): lax.psum_scatter(jnp.dot(branch, w_out_rows, preferred_element_type=jnp.f...]
    pallas_call x0 -> x1, Pallas kernels: none -> 29.2 us  [attend(): pl.pallas_call(functools.partial(attention_kernel, inner=inner, head_dim=...]
    all_to_all x0 -> x2, waiting for transfers between devices: none -> 25.8 us  [exchanged(): lax.all_to_all(blocks, 'sp', split_axis=0, concat_axis=0, tiled=True, axi...]
    all_to_all x0 -> x1, blocking collectives: none -> 23.9 us  [exchanged(): lax.all_to_all(blocks, 'sp', split_axis=0, concat_axis=0, tiled=True, axi...]
    ppermute x0 -> x2, waiting for transfers between devices: none -> 18.2 us  [swapped(): return lax.ppermute(block, axis, [(0, 1), (1, 0)])]
    all_gather x1, blocking collectives: 5.5 us -> 17.9 us  [local(): gains = lax.all_gather(gain_row, 'tp', axis=1, tiled=True)]
    all_gather x1 -> x0, local copies, waits for them, and re-layouts: 8.7 us -> none  [local(): lax.all_gather(key_rows, 'sp', axis=0, tiled=True)]
  transfers between devices with their start and end apart: 7 -> 8, of which waited for: 7 -> 6; matrix products, arithmetic and copies ran while one was open for 9% -> 5% of each run, Pallas kernels for 0% -> 12%
where the time goes in v1:
time: 240 us; the launch traced here: 239 us
  waiting for transfers between devices  113 us (47%)
  blocking collectives  41.9 us (17%)
  Pallas kernels  29.2 us (12%)
  matrix products  16.2 us (7%)
  starting transfers between devices  14 us (6%)
  between operations  13.3 us (6%)
  other arithmetic  6.11 us (3%)
  local copies, waits for them, and re-layouts  5.14 us (2%)
    all_gather x1, waiting for transfers between devices, local(): w_in_full = lax.all_gather(w_cat, 'sp', axis=0, tiled=True)  55 us
    pallas_call x1, Pallas kernels, attend(): pl.pallas_call(functools.partial(attention_kernel, inner=inner, head_dim=...  29.2 us
    all_to_all x2, waiting for transfers between devices, exchanged(): lax.all_to_all(blocks, 'sp', split_axis=0, concat_axis=0, tiled=True, axi...  25.8 us
    all_to_all x1, blocking collectives, exchanged(): lax.all_to_all(blocks, 'sp', split_axis=0, concat_axis=0, tiled=True, axi...  23.9 us
    ppermute x2, waiting for transfers between devices, swapped(): return lax.ppermute(block, axis, [(0, 1), (1, 0)])  18.2 us
    all_gather x1, blocking collectives, local(): gains = lax.all_gather(gain_row, 'tp', axis=1, tiled=True)  17.9 us
    all_gather x1, waiting for transfers between devices, local(): w_out_t = lax.all_gather(w_out.T, 'sp', axis=0, tiled=True)  8.9 us
    all_to_all x2, starting transfers between devices, exchanged(): lax.all_to_all(blocks, 'sp', split_axis=0, concat_axis=0, tiled=True, axi...  8.08 us
  transfers between devices with their start and end apart: 8, of which 6 were waited for; matrix products, arithmetic and copies ran while one was open for 5% of the time, Pallas kernels for 12%

profile of v1, /device:TPU:0, one launch (start us, length us, event | category | flops | bytes accessed | tf_op | source)
XLA Modules:
  0.0 239.0 jit_solution(7494418792658308751)
XLA Ops:
  6.5 2.0 pad_maximum_fusion.2
  8.6 3.0 %collective-permute-start = (bf16[384,1024]{1,0:T(8,128)(2,1)}, bf16[384,1024]{1,0:T(8,128)(2,1)S(1)}, u32[]{:S(2)}, u32[]{:S(2)}) collective-permute-start(bf16[384,1024]{1,0:T(8,128)(2,1)} %param.11), channel_id=1, source_target_pairs={{0,1},{1,0},{2,3},{3,2},{4,5},{5,4},{6,7},{7,6},{8,9},{9,8},{10,11... | collective-permute-start | bytes 2359304 | tf_op jit(solution)/shard_map/ppermute | solution.py:24
  11.7 17.9 %all-gather = bf16[2048]{0:T(1024)(128)(2,1)S(1)} all-gather(bf16[1024]{0:T(1024)(128)(2,1)} %param.12), channel_id=2, replica_groups=mesh['sp'=16,'tp'=2] {'tp'}, dimensions={0}, use_global_device_ids=true | all-gather | bytes 6144 | tf_op jit(solution)/shard_map/all_gather | solution.py:169
  29.6 1.9 fusion.1
  31.5 55.0 %all-gather.5.cloned.1.call-done = bf16[2048,2048]{1,0:T(8,128)(2,1)} async-done(((bf16[128,2048]{1,0:T(8,128)(2,1)}), bf16[2048,2048]{1,0:T(8,128)(2,1)}) %all-gather.5.cloned.1.call-update) | async-done | bytes 8388624 | tf_op jit(solution)/shard_map/all_gather | solution.py:158
  86.6 6.8 %multiply_convert_fusion = bf16[384,2048]{1,0:T(8,128)(2,1)S(1)} fusion(bf16[2048,2048]{1,0:T(8,128)(2,1)} %all-gather.5.cloned.1.call-done, f32[2048]{0:T(1024)S(1)} %mul.62, f32[384]{0:T(512)S(1)} %add_rsqrt_fusion, bf16[384,1024]{1,0:T(8,128)(2,1)S(1)} %collective-permute-done, bf16[384,1024]{1,0:T(8,128)(2,1)S(1)} %copy-done.1, pred[]{:T(512)S(6)} %eq.63), kind=kOutput, calls=%fused_computation.4 | convolution fusion | flops 3232235520 | bytes 11544065 | tf_op jit(solution)/shard_map/dot_general | solution.py:174
  93.3 0.2 fusion.34
  93.8 23.9 %all_to_all.15 = bf16[4,384,256]{2,1,0:T(8,128)(2,1)} all-to-all(bf16[4,384,256]{2,1,0:T(8,128)(2,1)S(1)} %pad_maximum_fusion), channel_id=1, replica_groups={{0,8,16,24},{2,10,18,26},{4,12,20,28},{6,14,22,30},{1,9,17,25},{3,11,19..., dimensions={0} | all-to-all | bytes 1572864 | tf_op jit(solution)/shard_map/all_to_all | solution.py:121
  117.9 0.7 all-gather.9.cloned.1.call-update
  118.6 0.6 dynamic_slice.9.lam_ref
  119.2 0.6 broadcast_bitcast_fusion
  119.8 0.7 broadcast_bitcast_fusion.1
  120.5 0.6 broadcast_bitcast_fusion.2
  121.1 0.6 broadcast_bitcast_fusion.3
  121.8 1.3 collective-permute-start.1
  123.1 0.8 pad_maximum_fusion.3
  123.9 3.5 %all-to-all-start = ((bf16[4,384,128]{2,1,0:T(8,128)(2,1)}), bf16[4,384,128]{2,1,0:T(8,128)(2,1)S(1)}, u32[]{:S(2)}, u32[]{:S(2)}) async-start(bf16[4,384,128]{2,1,0:T(8,128)(2,1)} %pad_maximum_fusion.3), calls=%async_computation | async-start | bytes 786432 | tf_op jit(solution)/shard_map/all_to_all | solution.py:121
  127.7 0.7 fusion.6
  128.5 0.3 copy.24
  128.9 1.0 slice.113
  129.8 10.3 %all-to-all-done = bf16[4,384,128]{2,1,0:T(8,128)(2,1)S(1)} async-done(((bf16[4,384,128]{2,1,0:T(8,128)(2,1)}), bf16[4,384,128]{2,1,0:T(8,128)(2,1)S(1)}, u32[]{:S(2)}, u32[]{:S(2)}) %all-to-all-start) | async-done | bytes 393248 | tf_op jit(solution)/shard_map/all_to_all | solution.py:121
  140.1 4.5 %all-gather.7.cloned.1.call-done = bf16[6144,256]{1,0:T(8,128)(2,1)} async-done(((bf16[1536,256]{1,0:T(8,128)(2,1)}), bf16[6144,256]{1,0:T(8,128)(2,1)}) %all-gather.7.cloned.1.call-update) | async-done | bytes 3145744 | tf_op jit(solution)/shard_map/all_gather | solution.py:196
  144.6 29.2 %diff_attention.1 = bf16[4,1,384,128]{3,2,1,0:T(8,128)(2,1)} custom-call(s32[1]{0:T(128)} %bitcast.place_ref, f32[1]{0:T(128)} %dynamic_slice.9.lam_ref, f32[1,128]{1,0:T(1,128)} %bitcast.74, bf16[4,1,384,128]{3,2,1,0:T(8,128)(2,1)} %bitcast.68, bf16[4,4,1,384,256]{4,3,2,1,0:T(8,128)(2,1)} %bitcast.72), custom_call_target="tpu_custom_call" | custom-call | flops 9663676416 | bytes 3145728 | tf_op jit(solution)/shard_map/diff_attention/pallas_call | solution.py:92
  173.8 4.6 %all-to-all-start.2 = ((bf16[4,384,128]{2,1,0:T(8,128)(2,1)}), bf16[4,384,128]{2,1,0:T(8,128)(2,1)S(1)}, u32[]{:S(2)}, u32[]{:S(2)}) async-start(bf16[4,384,128]{2,1,0:T(8,128)(2,1)} %bitcast.69), calls=%async_computation.2 | async-start | bytes 786432 | tf_op jit(solution)/shard_map/all_to_all | solution.py:121
  178.4 2.0 fusion.5
  180.4 15.5 %all-to-all-done.2 = bf16[4,384,128]{2,1,0:T(8,128)(2,1)S(1)} async-done(((bf16[4,384,128]{2,1,0:T(8,128)(2,1)}), bf16[4,384,128]{2,1,0:T(8,128)(2,1)S(1)}, u32[]{:S(2)}, u32[]{:S(2)}) %all-to-all-start.2) | async-done | bytes 393248 | tf_op jit(solution)/shard_map/all_to_all | solution.py:121
  196.0 0.4 copy.28
  196.4 8.9 %all-gather.9.cloned.1.call-done = bf16[2048,1024]{0,1:T(8,128)(2,1)} async-done(((bf16[128,1024]{0,1:T(8,128)(2,1)}), bf16[2048,1024]{0,1:T(8,128)(2,1)}) %all-gather.9.cloned.1.call-update) | async-done | bytes 4194320 | tf_op jit(solution)/shard_map/all_gather | solution.py:233
  205.3 3.3 %convolution_convert_fusion = bf16[192,2048]{1,0:T(8,128)(2,1)S(1)} fusion(bf16[2048,1024]{0,1:T(8,128)(2,1)} %all-gather.9.cloned.1.call-done, bf16[384,1024]{0,1:T(8,128)(2,1)S(1)} %bitcast.59, s32[]{:T(128)S(6)} %select_n.58), kind=kOutput, calls=%fused_computation.5 | convolution fusion | flops 805699584 | bytes 5505028 | tf_op jit(solution)/shard_map/dot_general | solution.py:236
  208.6 1.5 collective-permute-start.2
  210.1 18.2 %collective-permute-done.2 = bf16[192,2048]{1,0:T(8,128)(2,1)S(1)} collective-permute-done((bf16[192,2048]{1,0:T(8,128)(2,1)S(1)}, bf16[192,2048]{1,0:T(8,128)(2,1)S(1)}, u32[]{:S(2)}, u32[]{:S(2)}) %collective-permute-start.2) | collective-permute-done | bytes 786464 | tf_op jit(solution)/shard_map/ppermute | solution.py:24
  228.3 4.2 %add_convert_fusion = bf16[192,2048]{1,0:T(8,128)(2,1)} fusion(bf16[192,2048]{1,0:T(8,128)(2,1)S(1)} %collective-permute-done.2, bf16[2048,1024]{0,1:T(8,128)(2,1)} %all-gather.9.cloned.1.call-done, bf16[384,1024]{0,1:T(8,128)(2,1)S(1)} %bitcast.60, s32[]{:T(128)S(6)} %select_n.57), kind=kOutput, calls=%fused_computation.8 | convolution fusion | flops 806486016 | bytes 6291460 | tf_op jit(solution)/shard_map/dot_general | solution.py:236
  (35 shorter events, 0.9 us)
Async XLA Ops:
  6.5 171.9 %copy-start = (bf16[4,128,128]{2,1,0:T(8,128)(2,1)S(1)}, bf16[4,128,128]{2,1,0:T(8,128)(2,1)}, u32[]{:S(2)}) copy-start(bf16[4,128,128]{2,1,0:T(8,128)(2,1)} %param.19) | copy-start | bytes 393220
  6.5 80.0 %copy-start.1 = (bf16[384,1024]{1,0:T(8,128)(2,1)S(1)}, bf16[384,1024]{1,0:T(8,128)(2,1)}, u32[]{:S(2)}) copy-start(bf16[384,1024]{1,0:T(8,128)(2,1)} %param.11) | copy-start | bytes 2359300
  6.5 80.0 %all-gather.5.cloned.1.call-start = ((), (), s32[]{:S(2)}) async-start(), calls=%async_computation.3 | async-start | bytes 8912896 | tf_op jit(solution)/shard_map/all_gather | solution.py:158
  8.6 136.0 %all-gather.7.cloned.1.call-start = ((), (), s32[]{:S(2)}) async-start(), calls=%async_computation.4 | async-start | bytes 3932160 | tf_op jit(solution)/shard_map/all_gather | solution.py:196
  8.6 21.0 %collective-permute-start = (bf16[384,1024]{1,0:T(8,128)(2,1)}, bf16[384,1024]{1,0:T(8,128)(2,1)S(1)}, u32[]{:S(2)}, u32[]{:S(2)}) collective-permute-start(bf16[384,1024]{1,0:T(8,128)(2,1)} %param.11), channel_id=1, source_target_pairs={{0,1},{1,0},{2,3},{3,2},{4,5},{5,4},{6,7},{7,6},{8,9},{9,8},{10,11... | collective-permute-start | bytes 2359304 | tf_op jit(solution)/shard_map/ppermute | solution.py:24
  93.6 25.0 %copy-start.3 = (f32[4]{0:T(128)S(1)}, f32[4]{0:T(128)}, u32[]{:S(2)}) copy-start(f32[4]{0:T(128)} %param.17) | copy-start | bytes 52
  117.8 87.5 %all-gather.9.cloned.1.call-start = ((), (), s32[]{:S(2)}) async-start(), calls=%async_computation.5 | async-start | bytes 4456448 | tf_op jit(solution)/shard_map/all_gather | solution.py:233
  121.8 5.6 %collective-permute-start.1 = (bf16[15,512]{1,0:T(8,128)(2,1)S(1)}, bf16[15,512]{1,0:T(8,128)(2,1)S(1)}, u32[]{:S(2)}, u32[]{:S(2)}) collective-permute-start(bf16[15,512]{1,0:T(8,128)(2,1)S(1)} %slice.105), channel_id=1, source_target_pairs={{0,2},{2,4},{4,6},{6,8},{8,10},{10,12},{12,14},{14,16},{16,18},{18... | collective-permute-start | bytes 46088 | tf_op jit(solution)/shard_map/ppermute | solution.py:20
  123.9 16.2 %all-to-all-start = ((bf16[4,384,128]{2,1,0:T(8,128)(2,1)}), bf16[4,384,128]{2,1,0:T(8,128)(2,1)S(1)}, u32[]{:S(2)}, u32[]{:S(2)}) async-start(bf16[4,384,128]{2,1,0:T(8,128)(2,1)} %pad_maximum_fusion.3), calls=%async_computation | async-start | bytes 786432 | tf_op jit(solution)/shard_map/all_to_all | solution.py:121
  140.1 4.5 %copy-start.2 = (bf16[4,384,128]{2,1,0:T(8,128)(2,1)}, bf16[4,384,128]{2,1,0:T(8,128)(2,1)S(1)}, u32[]{:S(2)}) copy-start(bf16[4,384,128]{2,1,0:T(8,128)(2,1)S(1)} %all-to-all-done) | copy-start | bytes 1179652
  173.8 22.1 %all-to-all-start.2 = ((bf16[4,384,128]{2,1,0:T(8,128)(2,1)}), bf16[4,384,128]{2,1,0:T(8,128)(2,1)S(1)}, u32[]{:S(2)}, u32[]{:S(2)}) async-start(bf16[4,384,128]{2,1,0:T(8,128)(2,1)} %bitcast.69), calls=%async_computation.2 | async-start | bytes 786432 | tf_op jit(solution)/shard_map/all_to_all | solution.py:121
  208.6 19.8 %collective-permute-start.2 = (bf16[192,2048]{1,0:T(8,128)(2,1)S(1)}, bf16[192,2048]{1,0:T(8,128)(2,1)S(1)}, u32[]{:S(2)}, u32[]{:S(2)}) collective-permute-start(bf16[192,2048]{1,0:T(8,128)(2,1)S(1)} %convolution_convert_fusion), channel_id=1, source_target_pairs={{0,1},{1,0},{2,3},{3,2},{4,5},{5,4},{6,7},{7,6},{8,9},{9,8},{10,11... | collective-permute-start | bytes 2359304 | tf_op jit(solution)/shard_map/ppermute | solution.py:24
Sparse Core Ops, SparseCore 0:
  9.5 77.0 all-gather.4
  117.9 26.6 all-gather.6
  146.8 58.4 all-gather.8

commit v2 on v1

--- a/solution.py
+++ b/solution.py
@@ -24,55 +24,75 @@
     return lax.ppermute(block, axis, [(0, 1), (1, 0)])
 
 
-def attention_kernel(
-    place_ref, lam_ref, gain_ref, q_ref, kv_ref, out_ref, max_ref, acc_ref, *, inner, head_dim
-):
+def attention_kernel(place_ref, lam_ref, gain_ref, q_ref, *refs, inner, head_dim, parts):
+    key_refs = refs[:parts]
+    value_refs = refs[parts : 2 * parts]
+    out_ref, both_ref, max_ref, acc_ref = refs[2 * parts :]
     rows = q_ref.shape[2]
     value_dim = out_ref.shape[3]
     pair = 2 * head_dim
+    step_rows = math.gcd(rows, 128)
     scale = math.log2(math.e) / math.sqrt(head_dim)
-    query_block = pl.program_id(1) * inner + place_ref[0]
+    mine = place_ref[0]
+    query_block = pl.program_id(1) * inner + mine
     query = q_ref[0, 0]
     lane = lax.broadcasted_iota(jnp.int32, (rows, pair), 1)
     blank = jnp.zeros_like(query)
-    both = jnp.concatenate(
-        [jnp.where(lane < head_dim, query, blank), jnp.where(lane < head_dim, blank, query)], axis=0
-    )
-    ones = jnp.ones((rows, value_dim), jnp.bfloat16)
-
-    def scores_of(block):
-        keys = kv_ref[block % inner, block // inner, 0, :, :pair]
-        return scale * lax.dot_general(
-            both, keys, (((1,), (1,)), ((), ())), preferred_element_type=jnp.float32
-        )
-
-    def weighted_of(block, expo):
-        values = kv_ref[block % inner, block // inner, 0, :, pair:]
-        return jnp.dot(
-            expo.astype(jnp.bfloat16),
-            jnp.concatenate([values, ones], axis=1),
-            preferred_element_type=jnp.float32,
-        )
-
-    scores = scores_of(query_block)
-    row = lax.broadcasted_iota(jnp.int32, scores.shape, 0)
-    column = lax.broadcasted_iota(jnp.int32, scores.shape, 1)
-    row = jnp.where(row >= rows, row - rows, row)
-    scores = jnp.where(column <= row, scores, NEG_LARGE)
-    first_max = jnp.max(scores, axis=1, keepdims=True)
-    max_ref[...] = jnp.broadcast_to(first_max, max_ref.shape)
-    acc_ref[...] = weighted_of(query_block, jnp.exp2(scores - first_max))
-
-    def step(block, carry):
-        scores = scores_of(block)
-        old_max = max_ref[:, :1]
-        new_max = jnp.maximum(old_max, jnp.max(scores, axis=1, keepdims=True))
-        expo = jnp.exp2(scores - new_max)
-        max_ref[...] = jnp.broadcast_to(new_max, max_ref.shape)
-        acc_ref[...] = acc_ref[...] * jnp.exp2(old_max - new_max) + weighted_of(block, expo)
+    both_ref[:rows] = jnp.where(lane < head_dim, query, blank)
+    both_ref[rows:] = jnp.where(lane < head_dim, blank, query)
+    ones = jnp.ones((parts * rows, value_dim), jnp.bfloat16)
+
+    def masked(scores, start, group):
+        pieces = []
+        for part in range(parts):
+            block = group * parts + ((mine ^ part) if parts > 1 else 0)
+            piece = scores[:, part * rows : (part + 1) * rows]
+            row = lax.broadcasted_iota(jnp.int32, piece.shape, 0)
+            column = lax.broadcasted_iota(jnp.int32, piece.shape, 1)
+            ahead = (block - query_block) * rows - start % rows
+            pieces.append(jnp.where(column + ahead <= row, piece, NEG_LARGE))
+        return jnp.concatenate(pieces, axis=1)
+
+    def run_group(group, first):
+        keys = jnp.concatenate([ref[group, 0] for ref in key_refs], axis=0)
+        values = jnp.concatenate([ref[group, 0] for ref in value_refs], axis=0)
+        values = jnp.concatenate([values, ones], axis=1)
+
+        def scores_of(start):
+            return lax.dot_general(
+                both_ref[start : start + step_rows],
+                keys,
+                (((1,), (1,)), ((), ())),
+                preferred_element_type=jnp.float32,
+            )
+
+        coming = scores_of(0)
+        for start in range(0, 2 * rows, step_rows):
+            scores = coming * scale
+            if start + step_rows < 2 * rows:
+                coming = scores_of(start + step_rows)
+            here = slice(start, start + step_rows)
+            if first:
+                scores = masked(scores, start, group)
+            new_max = jnp.max(scores, axis=1, keepdims=True)
+            if not first:
+                old_max = max_ref[here, :1]
+                new_max = jnp.maximum(old_max, new_max)
+            expo = jnp.exp2(scores - new_max).astype(jnp.bfloat16)
+            weighted = jnp.dot(expo, values, preferred_element_type=jnp.float32)
+            if not first:
+                weighted = weighted + acc_ref[here] * jnp.exp2(old_max - new_max)
+            max_ref[here] = jnp.broadcast_to(new_max, (step_rows, max_ref.shape[1]))
+            acc_ref[here] = weighted
+
+    last = query_block // parts
+    run_group(last, True)
+
+    def step(group, carry):
+        run_group(group, False)
         return carry
 
-    lax.fori_loop(0, query_block, step, 0)
+    lax.fori_loop(0, last, step, 0)
     head_mix = (
         acc_ref[:rows, :value_dim] / acc_ref[:rows, value_dim:]
         - lam_ref[pl.program_id(0)]
@@ -84,24 +104,31 @@
     out_ref[0, 0] = normed.astype(jnp.bfloat16)
 
 
-def attend(place, lam, gain, queries, kv, head_dim):
-    spread, heads, rows, _ = queries.shape
-    inner = kv.shape[0]
-    value_dim = kv.shape[4] - 2 * head_dim
+def attend(place, lam, gain, queries, keys, values, inner, head_dim):
+    spread, heads, rows, pair = queries.shape
+    value_dim = values[0].shape[3]
     smem = pl.BlockSpec(memory_space=pltpu.SMEM)
+
+    def whole_head(array):
+        blocks, _, length, width = array.shape
+        return pl.BlockSpec((blocks, 1, length, width), lambda h, j: (0, h, 0, 0))
+
     return pl.pallas_call(
-        functools.partial(attention_kernel, inner=inner, head_dim=head_dim),
+        functools.partial(
+            attention_kernel, inner=inner, head_dim=head_dim, parts=len(keys)
+        ),
         grid=(heads, spread),
         in_specs=[
             smem,
             smem,
             pl.BlockSpec((1, value_dim), lambda h, j: (0, 0)),
-            pl.BlockSpec((1, 1, rows, 2 * head_dim), lambda h, j: (j, h, 0, 0)),
-            pl.BlockSpec((inner, spread, 1, rows, kv.shape[4]), lambda h, j: (0, 0, h, 0, 0)),
+            pl.BlockSpec((1, 1, rows, pair), lambda h, j: (j, h, 0, 0)),
+            *[whole_head(array) for array in (*keys, *values)],
         ],
         out_specs=pl.BlockSpec((1, 1, rows, value_dim), lambda h, j: (j, h, 0, 0)),
         out_shape=jax.ShapeDtypeStruct((spread, heads, rows, value_dim), jnp.bfloat16),
         scratch_shapes=[
+            pltpu.VMEM((2 * rows, pair), jnp.bfloat16),
             pltpu.VMEM((2 * rows, 128), jnp.float32),
             pltpu.VMEM((2 * rows, 2 * value_dim), jnp.float32),
         ],
@@ -111,16 +138,34 @@
         cost_estimate=pl.CostEstimate(
             flops=spread * heads * rows * rows * inner * spread * 1024,
             transcendentals=spread * heads * rows * rows * inner * spread,
-            bytes_accessed=kv.size * 2,
+            bytes_accessed=sum(array.size * 2 for array in (*keys, *values)),
         ),
         name="diff_attention",
-    )(place, lam, gain, queries, kv)
+    )(place, lam, gain, queries, *keys, *values)
 
 
 def exchanged(blocks, groups):
     return lax.all_to_all(
         blocks, "sp", split_axis=0, concat_axis=0, tiled=True, axis_index_groups=groups
     )
+
+
+def mirrored(block, bit):
+    return lax.ppermute(block, "sp", [(i, i ^ bit) for i in range(lax.axis_size("sp"))])
+
+
+def from_beside(block, inner, spread, groups):
+    if inner & (inner - 1) == 0 and inner <= 4:
+        held = [block]
+        bit = inner // 2
+        while bit > 0:
+            held = held + [mirrored(piece, bit) for piece in held]
+            bit //= 2
+        width = inner.bit_length() - 1
+        order = [int(format(t, "b").zfill(width)[::-1], 2) if width else 0 for t in range(inner)]
+        return [held[order[t]] for t in range(inner)]
+    full = lax.all_gather(block, "sp", axis=0, axis_index_groups=groups)
+    return [jnp.swapaxes(full, 0, 1).reshape(inner * spread, *block.shape[1:])]
 
 
 def local(
@@ -156,6 +201,7 @@
     my_tp = lax.axis_index("tp")
     w_cat = jnp.concatenate([w_query, w_key, w_value, w_pool], axis=1)
     w_in_full = lax.all_gather(w_cat, "sp", axis=0, tiled=True)
+    w_out_t = lax.all_gather(w_out.T, "sp", axis=0, tiled=True)
     gain_row = pre_gain.reshape(1, -1)
     if tp_size == 2:
         other = swapped(tokens, "tp")
@@ -174,31 +220,30 @@
     projection = jnp.dot(scaled, w_in_full, preferred_element_type=jnp.float32)
     projected = (projection * inverse[:, None]).astype(jnp.bfloat16)
     pair = 2 * head_dim
-    queries = jnp.stack([projected[:, h * pair : (h + 1) * pair] for h in range(local_heads)])
-    kv = jnp.stack(
-        [
-            jnp.concatenate(
-                [
-                    projected[:, q_cols + h * pair : q_cols + (h + 1) * pair],
-                    projected[:, 2 * q_cols + h * value_dim : 2 * q_cols + (h + 1) * value_dim],
-                ],
-                axis=1,
-            )
-            for h in range(local_heads)
-        ]
-    )
+
+    def by_head(first, width):
+        return jnp.stack(
+            [projected[:, first + h * width : first + (h + 1) * width] for h in range(local_heads)]
+        )
+
+    keys = by_head(q_cols, pair)
+    values = by_head(2 * q_cols, value_dim)
+    queries = by_head(0, pair)
     pool_in = projected[:, 2 * q_cols + v_cols :]
     positions = my_sp * tok_rows + jnp.arange(tok_rows, dtype=jnp.int32)
     if spread > 1:
-        kv = exchanged(kv, apart)
+        keys = exchanged(keys, apart)
+        values = exchanged(values, apart)
         queries = exchanged(queries, apart)
-    kv = kv.reshape(-1, kv.shape[2])
-    kv = lax.all_gather(kv, "sp", axis=0, tiled=True, axis_index_groups=beside)
-    kv = kv.reshape(inner, spread, heads_here, tok_rows, pair + value_dim)
-    queries = queries.reshape(spread, heads_here, tok_rows, pair)
+    shape = (spread, heads_here, tok_rows)
+    keys = from_beside(keys.reshape(*shape, pair), inner, spread, beside)
+    values = from_beside(values.reshape(*shape, value_dim), inner, spread, beside)
+    queries = queries.reshape(*shape, pair)
     lam = lax.dynamic_slice_in_dim(lambdas, (my_sp // inner) * heads_here, heads_here)
     place = (my_sp % inner).astype(jnp.int32).reshape(1)
-    attention = attend(place, lam, sub_gain.reshape(1, -1), queries, kv, head_dim)
+    attention = attend(
+        place, lam, sub_gain.reshape(1, -1), queries, keys, values, inner, head_dim
+    )
     attention = attention.reshape(local_heads, tok_rows, value_dim)
     if spread > 1:
         attention = exchanged(attention, apart)
@@ -230,7 +275,6 @@
     pooled = jnp.einsum("tgc,gcd->tgd", differ, group_weight, preferred_element_type=jnp.float32)
     pooled = (pooled * pool_scale.reshape(local_groups, group_dim)).astype(jnp.bfloat16)
     branch = jnp.concatenate([attention, pooled], axis=2).reshape(tok_rows, -1)
-    w_out_t = lax.all_gather(w_out.T, "sp", axis=0, tiled=True)
 
     def out_of(rows):
         return lax.dot_general(
@@ -241,7 +285,9 @@
         half = tok_rows // 2
         sent = out_of(lax.dynamic_slice_in_dim(branch, (1 - my_tp) * half, half))
         arrived = swapped(sent.astype(jnp.bfloat16), "tp")
-        kept = out_of(lax.dynamic_slice_in_dim(branch, my_tp * half, half))
+        kept = lax.optimization_barrier(
+            out_of(lax.dynamic_slice_in_dim(branch, my_tp * half, half))
+        )
         return (kept + arrived.astype(jnp.float32)).astype(jnp.bfloat16)
     return lax.psum_scatter(
         out_of(branch).astype(jnp.bfloat16), "tp", scatter_dimension=0, tiled=True

time: 240 us -> 228 us (0.950)
  blocking collectives: 41.9 us -> 17.9 us
  starting transfers between devices: 14 us -> 26.4 us
  Pallas kernels: 29.2 us -> 24.2 us
  other arithmetic: 6.11 us -> 10.5 us
    all_to_all x1 -> x0, blocking collectives: 23.9 us -> none  [exchanged(): lax.all_to_all(blocks, 'sp', split_axis=0, concat_axis=0, tiled=True, axi...]
    all_to_all x2 -> x4, waiting for transfers between devices: 25.8 us -> 41.2 us  [exchanged(): lax.all_to_all(blocks, 'sp', split_axis=0, concat_axis=0, tiled=True, axi...]
    all_gather x1, waiting for transfers between devices: 8.9 us -> 0.02 us  [local(): w_out_t = lax.all_gather(w_out.T, 'sp', axis=0, tiled=True)]
    all_to_all x2 -> x4, starting transfers between devices: 8.08 us -> 14.7 us  [exchanged(): lax.all_to_all(blocks, 'sp', split_axis=0, concat_axis=0, tiled=True, axi...]
    ppermute x0 -> x6, starting transfers between devices: none -> 5.88 us  [mirrored(): lax.ppermute(block, 'sp', [(i, i ^ bit) for i in range(lax.axis_size('sp'...]
    pallas_call x1, Pallas kernels: 29.2 us -> 24.2 us  [attend(): pl.pallas_call(functools.partial(attention_kernel, inner=inner, head_dim=...]
    all_gather x1 -> x0, waiting for transfers between devices: 4.5 us -> none  [local(): kv = lax.all_gather(kv, 'sp', axis=0, tiled=True, axis_index_groups=beside)]
    ppermute x0 -> x6, waiting for transfers between devices: none -> 4.25 us  [mirrored(): lax.ppermute(block, 'sp', [(i, i ^ bit) for i in range(lax.axis_size('sp'...]
  transfers between devices with their start and end apart: 8 -> 15, of which waited for: 6 -> 7; matrix products, arithmetic and copies ran while one was open for 5% -> 11% of each run, Pallas kernels for 12% -> 11%
where the time goes in v2:
time: 228 us
  waiting for transfers between devices  114 us (50%)
  starting transfers between devices  26.4 us (12%)
  Pallas kernels  24.2 us (11%)
  blocking collectives  17.9 us (8%)
  matrix products  15.3 us (7%)
  between operations  13.7 us (6%)
  other arithmetic  10.5 us (5%)
  local copies, waits for them, and re-layouts  5.64 us (2%)
    all_gather x1, waiting for transfers between devices, local(): w_in_full = lax.all_gather(w_cat, 'sp', axis=0, tiled=True)  53.7 us
    all_to_all x4, waiting for transfers between devices, exchanged(): lax.all_to_all(blocks, 'sp', split_axis=0, concat_axis=0, tiled=True, axi...  41.2 us
    pallas_call x1, Pallas kernels, attend(): pl.pallas_call(functools.partial(attention_kernel, inner=inner, head_dim=...  24.2 us
    all_gather x1, blocking collectives, local(): gains = lax.all_gather(gain_row, 'tp', axis=1, tiled=True)  17.9 us
    all_to_all x4, starting transfers between devices, exchanged(): lax.all_to_all(blocks, 'sp', split_axis=0, concat_axis=0, tiled=True, axi...  14.7 us
    ppermute x2, waiting for transfers between devices, swapped(): return lax.ppermute(block, axis, [(0, 1), (1, 0)])  14.1 us
    dot_general x1, matrix products, local(): projection = jnp.dot(scaled, w_in_full, preferred_element_type=jnp.float32)  6.79 us
    dot_general x2, matrix products, out_of(): lax.dot_general(rows, w_out_t, (((1,), (1,)), ((), ())), preferred_elemen...  6.55 us
  transfers between devices with their start and end apart: 15, of which 7 were waited for; matrix products, arithmetic and copies ran while one was open for 11% of the time, Pallas kernels for 11%

profile of v2, /device:TPU:0, one launch (start us, length us, event | category | flops | bytes accessed | tf_op | source)
XLA Modules:
  0.0 227.7 jit_solution(7718065203232884614)
XLA Ops:
  6.5 2.0 pad_maximum_fusion.1
  8.6 0.7 all-gather.6.cloned.1.call-update
  9.3 3.0 %collective-permute-start = (bf16[384,1024]{1,0:T(8,128)(2,1)}, bf16[384,1024]{1,0:T(8,128)(2,1)S(1)}, u32[]{:S(2)}, u32[]{:S(2)}) collective-permute-start(bf16[384,1024]{1,0:T(8,128)(2,1)} %param.11), channel_id=1, source_target_pairs={{0,1},{1,0},{2,3},{3,2},{4,5},{5,4},{6,7},{7,6},{8,9},{9,8},{10,11... | collective-permute-start | bytes 2359304 | tf_op jit(solution)/shard_map/ppermute | solution.py:24
  12.4 17.9 %all-gather = bf16[2048]{0:T(1024)(128)(2,1)S(1)} all-gather(bf16[1024]{0:T(1024)(128)(2,1)} %param.12), channel_id=2, replica_groups=mesh['sp'=16,'tp'=2] {'tp'}, dimensions={0}, use_global_device_ids=true | all-gather | bytes 6144 | tf_op jit(solution)/shard_map/all_gather | solution.py:215
  30.9 1.9 fusion.1
  32.8 53.7 %all-gather.4.cloned.1.call-done = bf16[2048,2048]{1,0:T(8,128)(2,1)} async-done(((bf16[128,2048]{1,0:T(8,128)(2,1)}), bf16[2048,2048]{1,0:T(8,128)(2,1)}) %all-gather.4.cloned.1.call-update) | async-done | bytes 8388624 | tf_op jit(solution)/shard_map/all_gather | solution.py:203
  86.6 6.8 %multiply_convert_fusion = bf16[384,2048]{1,0:T(8,128)(2,1)S(1)} fusion(bf16[2048,2048]{1,0:T(8,128)(2,1)} %all-gather.4.cloned.1.call-done, f32[2048]{0:T(1024)S(1)} %mul.62, f32[384]{0:T(512)S(1)} %add_rsqrt_fusion, bf16[384,1024]{1,0:T(8,128)(2,1)S(1)} %collective-permute-done, bf16[384,1024]{1,0:T(8,128)(2,1)S(1)} %copy-done.1, pred[]{:T(512)S(6)} %eq.63), kind=kOutput, calls=%fused_computation.4 | convolution fusion | flops 3232235520 | bytes 11544065 | tf_op jit(solution)/shard_map/dot_general | solution.py:220
  93.6 0.8 pad_maximum_fusion.4
  94.4 3.5 %all-to-all-start.2 = ((bf16[4,384,128]{2,1,0:T(8,128)(2,1)}), bf16[4,384,128]{2,1,0:T(8,128)(2,1)S(1)}, u32[]{:S(2)}, u32[]{:S(2)}) async-start(bf16[4,384,128]{2,1,0:T(8,128)(2,1)} %pad_maximum_fusion.4), calls=%async_computation.2 | async-start | bytes 786432 | tf_op jit(solution)/shard_map/all_to_all | solution.py:148
  99.1 0.8 pad_maximum_fusion.3
  99.9 16.0 %all-to-all-done.2 = bf16[4,384,128]{2,1,0:T(8,128)(2,1)S(1)} async-done(((bf16[4,384,128]{2,1,0:T(8,128)(2,1)}), bf16[4,384,128]{2,1,0:T(8,128)(2,1)S(1)}, u32[]{:S(2)}, u32[]{:S(2)}) %all-to-all-start.2) | async-done | bytes 393248 | tf_op jit(solution)/shard_map/all_to_all | solution.py:148
  115.9 3.5 %all-to-all-start.1 = ((bf16[4,384,128]{2,1,0:T(8,128)(2,1)}), bf16[4,384,128]{2,1,0:T(8,128)(2,1)S(1)}, u32[]{:S(2)}, u32[]{:S(2)}) async-start(bf16[4,384,128]{2,1,0:T(8,128)(2,1)} %pad_maximum_fusion.3), calls=%async_computation.1 | async-start | bytes 786432 | tf_op jit(solution)/shard_map/all_to_all | solution.py:148
  121.8 1.3 collective-permute-start.7
  123.1 0.8 pad_maximum_fusion.2
  123.9 2.1 collective-permute-start.5
  126.0 13.5 %all-to-all-done.1 = bf16[4,384,128]{2,1,0:T(8,128)(2,1)S(1)} async-done(((bf16[4,384,128]{2,1,0:T(8,128)(2,1)}), bf16[4,384,128]{2,1,0:T(8,128)(2,1)S(1)}, u32[]{:S(2)}, u32[]{:S(2)}) %all-to-all-start.1) | async-done | bytes 393248 | tf_op jit(solution)/shard_map/all_to_all | solution.py:148
  139.5 4.1 %all-to-all-start = ((bf16[4,384,128]{2,1,0:T(8,128)(2,1)}), bf16[4,384,128]{2,1,0:T(8,128)(2,1)}, u32[]{:S(2)}, u32[]{:S(2)}) async-start(bf16[4,384,128]{2,1,0:T(8,128)(2,1)} %pad_maximum_fusion.2), calls=%async_computation | async-start | bytes 786432 | tf_op jit(solution)/shard_map/all_to_all | solution.py:148
  143.7 3.2 %collective-permute-start.2 = (bf16[4,1,384,128]{3,2,0,1:T(8,128)(2,1)S(1)}, bf16[4,1,384,128]{3,2,0,1:T(8,128)(2,1)}, u32[]{:S(2)}, u32[]{:S(2)}) collective-permute-start(bf16[4,1,384,128]{3,2,0,1:T(8,128)(2,1)S(1)} %bitcast.85), channel_id=1, source_target_pairs={{0,4},{2,6},{4,0},{6,2},{8,12},{10,14},{12,8},{14,10},{16,20},{18,... | collective-permute-start | bytes 1179656 | tf_op jit(solution)/shard_map/ppermute | solution.py:154
  147.1 0.7 fusion.6
  148.5 4.2 %collective-permute-done.2 = bf16[4,1,384,128]{3,2,0,1:T(8,128)(2,1)} collective-permute-done((bf16[4,1,384,128]{3,2,0,1:T(8,128)(2,1)S(1)}, bf16[4,1,384,128]{3,2,0,1:T(8,128)(2,1)}, u32[]{:S(2)}, u32[]{:S(2)}) %collective-permute-start.2) | collective-permute-done | bytes 393248 | tf_op jit(solution)/shard_map/ppermute | solution.py:154
  153.3 0.7 reduce-window.9
  154.5 1.0 slice.113
  155.5 1.5 all-to-all-done
  157.1 24.2 %diff_attention.1 = bf16[4,1,384,128]{3,2,1,0:T(8,128)(2,1)} custom-call(s32[1]{0:T(128)} %bitcast.place_ref, f32[1]{0:T(128)} %dynamic_slice.9.lam_ref, f32[1,128]{1,0:T(1,128)} %bitcast.92, bf16[4,1,384,128]{3,2,1,0:T(8,128)(2,1)} %bitcast.7.q_ref, bf16[4,1,384,128]{3,2,1,0:T(8,128)(2,1)} %bitcast.87, bf16[4,1,384,128]{3,2,1,0:T(8,128)(2,1)} %bitcast.14.refs_1_, ...), custom_call_target="tpu_custom_call" | custom-call | flops 9663676416 | bytes 3145728 | tf_op jit(solution)/shard_map/diff_attention/pallas_call | solution.py:116
  181.3 3.6 %all-to-all-start.3 = ((bf16[4,384,128]{2,1,0:T(8,128)(2,1)}), bf16[4,384,128]{2,1,0:T(8,128)(2,1)S(1)}, u32[]{:S(2)}, u32[]{:S(2)}) async-start(bf16[4,384,128]{2,1,0:T(8,128)(2,1)} %bitcast.88), calls=%async_computation.3 | async-start | bytes 786432 | tf_op jit(solution)/shard_map/all_to_all | solution.py:148
  185.0 2.0 fusion.5
  187.0 10.1 %all-to-all-done.3 = bf16[4,384,128]{2,1,0:T(8,128)(2,1)S(1)} async-done(((bf16[4,384,128]{2,1,0:T(8,128)(2,1)}), bf16[4,384,128]{2,1,0:T(8,128)(2,1)S(1)}, u32[]{:S(2)}, u32[]{:S(2)}) %all-to-all-start.3) | async-done | bytes 393248 | tf_op jit(solution)/shard_map/all_to_all | solution.py:148
  197.6 3.3 %convolution_convert_fusion = bf16[192,2048]{1,0:T(8,128)(2,1)S(1)} fusion(bf16[2048,1024]{0,1:T(8,128)(2,1)} %all-gather.6.cloned.1.call-done, bf16[384,1024]{0,1:T(8,128)(2,1)S(1)} %bitcast.74, s32[]{:T(128)S(6)} %select_n.58), kind=kOutput, calls=%fused_computation.5 | convolution fusion | flops 805699584 | bytes 5505028 | tf_op jit(solution)/shard_map/dot_general | solution.py:280
  200.9 1.5 collective-permute-start.8
  202.4 3.3 %fusion.23 = f32[192,2048]{1,0:T(8,128)S(1)} fusion(bf16[2048,1024]{0,1:T(8,128)(2,1)} %all-gather.6.cloned.1.call-done, bf16[384,1024]{0,1:T(8,128)(2,1)S(1)} %bitcast.75, s32[]{:T(128)S(6)} %select_n.57), kind=kOutput, calls=%fused_computation.35 | convolution fusion | flops 805306368 | bytes 6291460 | tf_op jit(solution)/shard_map/dot_general | solution.py:280
  205.7 14.1 %collective-permute-done.8 = bf16[192,2048]{1,0:T(8,128)(2,1)S(1)} collective-permute-done((bf16[192,2048]{1,0:T(8,128)(2,1)S(1)}, bf16[192,2048]{1,0:T(8,128)(2,1)S(1)}, u32[]{:S(2)}, u32[]{:S(2)}) %collective-permute-start.8) | collective-permute-done | bytes 786464 | tf_op jit(solution)/shard_map/ppermute | solution.py:24
  219.8 1.1 add_convert_fusion
  (57 shorter events, 7.1 us)
Async XLA Ops:
  6.5 178.4 %copy-start = (bf16[4,128,128]{2,1,0:T(8,128)(2,1)S(1)}, bf16[4,128,128]{2,1,0:T(8,128)(2,1)}, u32[]{:S(2)}) copy-start(bf16[4,128,128]{2,1,0:T(8,128)(2,1)} %param.19) | copy-start | bytes 393220
  6.5 80.0 %copy-start.1 = (bf16[384,1024]{1,0:T(8,128)(2,1)S(1)}, bf16[384,1024]{1,0:T(8,128)(2,1)}, u32[]{:S(2)}) copy-start(bf16[384,1024]{1,0:T(8,128)(2,1)} %param.11) | copy-start | bytes 2359300
  6.5 80.0 %all-gather.4.cloned.1.call-start = ((), (), s32[]{:S(2)}) async-start(), calls=%async_computation.4 | async-start | bytes 8912896 | tf_op jit(solution)/shard_map/all_gather | solution.py:203
  8.6 189.0 %all-gather.6.cloned.1.call-start = ((), (), s32[]{:S(2)}) async-start(), calls=%async_computation.5 | async-start | bytes 4456448 | tf_op jit(solution)/shard_map/all_gather | solution.py:204
  9.3 21.6 %collective-permute-start = (bf16[384,1024]{1,0:T(8,128)(2,1)}, bf16[384,1024]{1,0:T(8,128)(2,1)S(1)}, u32[]{:S(2)}, u32[]{:S(2)}) collective-permute-start(bf16[384,1024]{1,0:T(8,128)(2,1)} %param.11), channel_id=1, source_target_pairs={{0,1},{1,0},{2,3},{3,2},{4,5},{5,4},{6,7},{7,6},{8,9},{9,8},{10,11... | collective-permute-start | bytes 2359304 | tf_op jit(solution)/shard_map/ppermute | solution.py:24
  93.3 26.7 %copy-start.8 = (f32[4]{0:T(128)S(1)}, f32[4]{0:T(128)}, u32[]{:S(2)}) copy-start(f32[4]{0:T(128)} %param.17) | copy-start | bytes 52
  94.4 21.5 %all-to-all-start.2 = ((bf16[4,384,128]{2,1,0:T(8,128)(2,1)}), bf16[4,384,128]{2,1,0:T(8,128)(2,1)S(1)}, u32[]{:S(2)}, u32[]{:S(2)}) async-start(bf16[4,384,128]{2,1,0:T(8,128)(2,1)} %pad_maximum_fusion.4), calls=%async_computation.2 | async-start | bytes 786432 | tf_op jit(solution)/shard_map/all_to_all | solution.py:148
  115.9 31.9 %copy-start.2 = (bf16[4,384,128]{2,1,0:T(8,128)(2,1)}, bf16[4,384,128]{2,1,0:T(8,128)(2,1)S(1)}, u32[]{:S(2)}) copy-start(bf16[4,384,128]{2,1,0:T(8,128)(2,1)S(1)} %all-to-all-done.2) | copy-start | bytes 1179652
  115.9 23.6 %all-to-all-start.1 = ((bf16[4,384,128]{2,1,0:T(8,128)(2,1)}), bf16[4,384,128]{2,1,0:T(8,128)(2,1)S(1)}, u32[]{:S(2)}, u32[]{:S(2)}) async-start(bf16[4,384,128]{2,1,0:T(8,128)(2,1)} %pad_maximum_fusion.3), calls=%async_computation.1 | async-start | bytes 786432 | tf_op jit(solution)/shard_map/all_to_all | solution.py:148
  121.8 25.0 %collective-permute-start.7 = (bf16[15,512]{1,0:T(8,128)(2,1)S(1)}, bf16[15,512]{1,0:T(8,128)(2,1)S(1)}, u32[]{:S(2)}, u32[]{:S(2)}) collective-permute-start(bf16[15,512]{1,0:T(8,128)(2,1)S(1)} %slice.105), channel_id=1, source_target_pairs={{0,2},{2,4},{4,6},{6,8},{8,10},{10,12},{12,14},{14,16},{16,18},{18... | collective-permute-start | bytes 46088 | tf_op jit(solution)/shard_map/ppermute | solution.py:20
  123.9 24.4 %collective-permute-start.5 = (bf16[4,1,384,128]{3,2,1,0:T(8,128)(2,1)S(1)}, bf16[4,1,384,128]{3,2,1,0:T(8,128)(2,1)}, u32[]{:S(2)}, u32[]{:S(2)}) collective-permute-start(bf16[4,1,384,128]{3,2,1,0:T(8,128)(2,1)S(1)} %bitcast.82), channel_id=1, source_target_pairs={{0,4},{2,6},{4,0},{6,2},{8,12},{10,14},{12,8},{14,10},{16,20},{18,... | collective-permute-start | bytes 1179656 | tf_op jit(solution)/shard_map/ppermute | solution.py:154
  139.5 14.5 %copy-start.3 = (bf16[4,384,128]{2,1,0:T(8,128)(2,1)}, bf16[4,384,128]{2,1,0:T(8,128)(2,1)S(1)}, u32[]{:S(2)}) copy-start(bf16[4,384,128]{2,1,0:T(8,128)(2,1)S(1)} %all-to-all-done.1) | copy-start | bytes 1179652
  139.5 17.5 %all-to-all-start = ((bf16[4,384,128]{2,1,0:T(8,128)(2,1)}), bf16[4,384,128]{2,1,0:T(8,128)(2,1)}, u32[]{:S(2)}, u32[]{:S(2)}) async-start(bf16[4,384,128]{2,1,0:T(8,128)(2,1)} %pad_maximum_fusion.2), calls=%async_computation | async-start | bytes 786432 | tf_op jit(solution)/shard_map/all_to_all | solution.py:148
  143.7 9.0 %collective-permute-start.2 = (bf16[4,1,384,128]{3,2,0,1:T(8,128)(2,1)S(1)}, bf16[4,1,384,128]{3,2,0,1:T(8,128)(2,1)}, u32[]{:S(2)}, u32[]{:S(2)}) collective-permute-start(bf16[4,1,384,128]{3,2,0,1:T(8,128)(2,1)S(1)} %bitcast.85), channel_id=1, source_target_pairs={{0,4},{2,6},{4,0},{6,2},{8,12},{10,14},{12,8},{14,10},{16,20},{18,... | collective-permute-start | bytes 1179656 | tf_op jit(solution)/shard_map/ppermute | solution.py:154
  147.8 9.2 %collective-permute-start.4 = (bf16[4,1,384,128]{3,2,1,0:T(8,128)(2,1)S(1)}, bf16[4,1,384,128]{3,2,1,0:T(8,128)(2,1)}, u32[]{:S(2)}, u32[]{:S(2)}) collective-permute-start(bf16[4,1,384,128]{3,2,1,0:T(8,128)(2,1)S(1)} %bitcast.83), channel_id=1, source_target_pairs={{0,2},{2,0},{4,6},{6,4},{8,10},{10,8},{12,14},{14,12},{16,18},{18,... | collective-permute-start | bytes 1179656 | tf_op jit(solution)/shard_map/ppermute | solution.py:154
  147.9 9.1 %collective-permute-start.1 = (bf16[4,1,384,128]{3,2,0,1:T(8,128)(2,1)S(1)}, bf16[4,1,384,128]{3,2,0,1:T(8,128)(2,1)}, u32[]{:S(2)}, u32[]{:S(2)}) collective-permute-start(bf16[4,1,384,128]{3,2,0,1:T(8,128)(2,1)S(1)} %bitcast.86), channel_id=1, source_target_pairs={{0,2},{2,0},{4,6},{6,4},{8,10},{10,8},{12,14},{14,12},{16,18},{18,... | collective-permute-start | bytes 1179656 | tf_op jit(solution)/shard_map/ppermute | solution.py:154
  148.4 8.6 %collective-permute-start.6 = (bf16[4,1,384,128]{3,2,1,0:T(8,128)(2,1)}, bf16[4,1,384,128]{3,2,1,0:T(8,128)(2,1)}, u32[]{:S(2)}, u32[]{:S(2)}) collective-permute-start(bf16[4,1,384,128]{3,2,1,0:T(8,128)(2,1)} %collective-permute-done.5.refs_6_), channel_id=1, source_target_pairs={{0,2},{2,0},{4,6},{6,4},{8,10},{10,8},{12,14},{14,12},{16,18},{18,... | collective-permute-start | bytes 1179656 | tf_op jit(solution)/shard_map/ppermute | solution.py:154
  152.7 4.3 %collective-permute-start.3 = (bf16[4,1,384,128]{3,2,0,1:T(8,128)(2,1)}, bf16[4,1,384,128]{3,2,0,1:T(8,128)(2,1)}, u32[]{:S(2)}, u32[]{:S(2)}) collective-permute-start(bf16[4,1,384,128]{3,2,0,1:T(8,128)(2,1)} %collective-permute-done.2), channel_id=1, source_target_pairs={{0,2},{2,0},{4,6},{6,4},{8,10},{10,8},{12,14},{14,12},{16,18},{18,... | collective-permute-start | bytes 1179656 | tf_op jit(solution)/shard_map/ppermute | solution.py:154
  157.0 27.9 %copy-start.4 = (f32[384]{0:T(512)S(1)}, f32[384]{0:T(512)}, u32[]{:S(2)}) copy-start(f32[384]{0:T(512)} %get-tuple-element.17) | copy-start | bytes 4612
  157.0 27.9 %copy-start.5 = (f32[384]{0:T(512)S(1)}, f32[384]{0:T(512)}, u32[]{:S(2)}) copy-start(f32[384]{0:T(512)} %get-tuple-element.18) | copy-start | bytes 4612
  157.0 27.9 %copy-start.6 = (f32[384]{0:T(512)S(1)}, f32[384]{0:T(512)}, u32[]{:S(2)}) copy-start(f32[384]{0:T(512)} %get-tuple-element.19) | copy-start | bytes 4612
  157.0 27.9 %copy-start.7 = (f32[384]{0:T(512)S(1)}, f32[384]{0:T(512)}, u32[]{:S(2)}) copy-start(f32[384]{0:T(512)} %get-tuple-element.20) | copy-start | bytes 4612
  181.3 15.8 %all-to-all-start.3 = ((bf16[4,384,128]{2,1,0:T(8,128)(2,1)}), bf16[4,384,128]{2,1,0:T(8,128)(2,1)S(1)}, u32[]{:S(2)}, u32[]{:S(2)}) async-start(bf16[4,384,128]{2,1,0:T(8,128)(2,1)} %bitcast.88), calls=%async_computation.3 | async-start | bytes 786432 | tf_op jit(solution)/shard_map/all_to_all | solution.py:148
  200.9 18.9 %collective-permute-start.8 = (bf16[192,2048]{1,0:T(8,128)(2,1)S(1)}, bf16[192,2048]{1,0:T(8,128)(2,1)S(1)}, u32[]{:S(2)}, u32[]{:S(2)}) collective-permute-start(bf16[192,2048]{1,0:T(8,128)(2,1)S(1)} %convolution_convert_fusion), channel_id=1, source_target_pairs={{0,1},{1,0},{2,3},{3,2},{4,5},{5,4},{6,7},{7,6},{8,9},{9,8},{10,11... | collective-permute-start | bytes 2359304 | tf_op jit(solution)/shard_map/ppermute | solution.py:24
Sparse Core Ops, SparseCore 0:
  9.5 77.0 all-gather.3
  88.7 69.6 all-gather.5
